TPU v7x, 256 devices: a whole 4x4x8 slice. The times are simulated.
256 devices in a mesh: ep: 16 (over y, x), tp: 16 (over z, core).
Axes of the slice: x: 4, y: 4, z: 8, core: 2. Of those that a mesh axis runs over, the one named last changes fastest.
Arguments:
- pool_input: bfloat16 [32768, 1024], P('ep', 'tp'), may hold values from -6 to 6
- pool_gain: float32 [1024], P('tp'), may hold values from 0.1 to 1.9
- mix_weight: bfloat16 [1024, 2048], P('tp'), may hold values from -0.1875 to 0.1875
- moe_input: bfloat16 [65536, 2048], P(('ep', 'tp')), may hold values from -6 to 6
- moe_gain: float32 [2048], replicated, may hold values from 0.1 to 1.9
- expert_ids: int32 [65536, 2], P(('ep', 'tp')), may hold values from 0 to 15, as said below
- route_weight: float32 [65536, 2], P(('ep', 'tp')), may hold values from 0.2 to 1
- gate_weight: bfloat16 [16, 2048, 1024], P('ep', None, 'tp'), may hold values from -0.125 to 0.125
- up_weight: bfloat16 [16, 2048, 1024], P('ep', None, 'tp'), may hold values from -0.125 to 0.125
- down_weight: bfloat16 [16, 2048, 1024], P('ep', None, 'tp'), may hold values from -0.1875 to 0.1875
Outputs:
- mixed_out: bfloat16 [32768, 2048], P(('ep', 'tp'))
- moe_out: bfloat16 [65536, 2048], P(('ep', 'tp'))
Inputs may be any that keep to these rules, and one draw needn't show every extreme that they name: `expert_ids`: each row names 2 different experts of one group of 4 consecutive experts. In each aligned block of 256 rows (the rows of one device) no expert is named by more than 48 rows, and some expert is named by exactly 48 rows.
All inputs are finite; a program needn't handle non-finite values.
Results may differ from a plain program's by a relative error of at most 0.012.
Values may be sent and summed in bfloat16 or wider, within the bound.
A program may use at most 128 MiB of HBM per device.

v0:
```python
import jax
import jax.numpy as jnp
from jax import lax
from jax.sharding import PartitionSpec as P

GROUP_CH = 256
EXPERTS = 16
TOP = 2
CAP = 48
eps_norm = 1e-06


def from_behind(shard, axis, by):
    peers = lax.axis_size(axis)
    pairs = [(i, i + by) for i in range(peers) if 0 <= i + by < peers]
    return lax.ppermute(shard, axis, pairs)


def gather_turned(arrays, axis, dims):
    turned = [jnp.moveaxis(a, dim, 0) for a, dim in zip(arrays, dims)]
    both = jnp.concatenate([t.reshape(len(t), -1) for t in turned], axis=1)
    result, at, gathered = (lax.all_gather(both, axis, axis=0, tiled=True), 0, [])
    for t, dim in zip(turned, dims):
        section = result[:, at : at + t[0].size].reshape(-1, *t.shape[1:])
        gathered.append(jnp.moveaxis(section, 0, dim))
        at += t[0].size
    return tuple(gathered)


def in_blocks(shard, dim, peers):
    before, after = (shard.shape[:dim], shard.shape[dim + 1 :])
    return jnp.moveaxis(shard.reshape(*before, peers, -1, *after), dim, 0)


def cut_rows(length, count):
    unit = 8 if length >= 8 * count else 1
    return [length // unit * k // count * unit for k in range(1, count)]


def joined_along(tiles, dim):
    tiles = jnp.moveaxis(tiles, 0, dim)
    dims = tiles.shape
    return tiles.reshape(*dims[:dim], dims[dim] * dims[dim + 1], *dims[dim + 2 :])


def exchange_in_pieces(shard, axis, pieces, split_dim, concat_dim):
    tiles = in_blocks(shard, split_dim, lax.axis_size(axis))
    widest = max(range(1, max(2, tiles.ndim - 1)), key=lambda d: tiles.shape[d])
    gathered = []
    for section in jnp.split(tiles, cut_rows(tiles.shape[widest], pieces), axis=widest):
        if section.size:
            gathered.append(lax.all_to_all(section, axis, split_axis=0, concat_axis=0, tiled=True))
    return joined_along(jnp.concatenate(gathered, axis=widest), concat_dim)


def window_sums(extended, row_count):
    level_sum = extended
    stride = 1
    outputs = []
    for doubling in range(4):
        level_sum = level_sum[stride:] + level_sum[:-stride]
        stride = stride * 2
        outputs.append(level_sum[level_sum.shape[0] - row_count :])
    return outputs


def pool_mixer(pool_input, pool_gain):
    row_count, channels = pool_input.shape
    carried = from_behind(pool_input[row_count - 15 :], "ep", 1)
    extended = jnp.concatenate([carried, pool_input], axis=0).astype(jnp.float32)
    window_list = window_sums(extended, row_count)
    channel_ids = lax.axis_index("tp") * channels + lax.iota(jnp.int32, channels)
    group_ids = channel_ids // GROUP_CH
    position = lax.axis_index("ep") * row_count + lax.iota(jnp.int32, row_count)
    summed = jnp.zeros((row_count, channels), jnp.float32)
    widths = jnp.zeros((channels,), jnp.int32)
    for index_group in range(4):
        inside = group_ids == index_group
        summed = jnp.where(inside[None, :], window_list[index_group], summed)
        widths = jnp.where(inside, 2 ** (index_group + 1), widths)
    counted = jnp.minimum(position[:, None] + 1, widths[None, :]).astype(jnp.float32)
    values = extended[15:]
    return ((summed / counted - values) * pool_gain).astype(jnp.bfloat16)


def route_slots(expert_ids):
    flat_ids = expert_ids.reshape(-1)
    marked = (flat_ids[:, None] == lax.iota(jnp.int32, EXPERTS)[None, :]).astype(jnp.int32)
    before_count = jnp.cumsum(marked, axis=0) - marked
    ranked = jnp.sum(before_count * marked, axis=1)
    return (flat_ids * CAP + ranked).reshape(expert_ids.shape)


def body(
    pool_input,
    pool_gain,
    mix_weight,
    moe_input,
    moe_gain,
    expert_ids,
    route_weight,
    gate_weight,
    up_weight,
    down_weight,
):
    pooled = pool_mixer(pool_input, pool_gain)
    mixed_sum = lax.psum_scatter(
        jnp.dot(pooled, mix_weight, preferred_element_type=jnp.float32).astype(jnp.bfloat16),
        "tp",
        scatter_dimension=0,
        tiled=True,
    )
    inputs = moe_input.astype(jnp.float32)
    scale_rows = lax.rsqrt(jnp.mean(inputs * inputs, axis=-1, keepdims=True) + eps_norm)
    normed = (inputs * scale_rows * moe_gain).astype(jnp.bfloat16)
    slots = route_slots(expert_ids)
    slot_index = lax.iota(jnp.int32, EXPERTS * CAP)
    placing = (
        (slot_index[:, None] == slots[None, :, 0]) | (slot_index[:, None] == slots[None, :, 1])
    ).astype(jnp.bfloat16)
    outgoing = jnp.dot(placing, normed, preferred_element_type=jnp.float32).astype(jnp.bfloat16)
    outgoing = outgoing.reshape(EXPERTS, CAP, normed.shape[1])
    arrived = lax.all_to_all(outgoing, "ep", split_axis=0, concat_axis=1, tiled=True)
    gate_piece, up_piece, down_piece = gather_turned(
        (gate_weight, up_weight, down_weight), "tp", (2, 2, 2)
    )
    gate_part = jnp.einsum("erd,edf->erf", arrived, gate_piece, preferred_element_type=jnp.float32)
    upward = jnp.einsum("erd,edf->erf", arrived, up_piece, preferred_element_type=jnp.float32)
    hidden = (jax.nn.silu(gate_part) * upward).astype(jnp.bfloat16)
    expert_sum = jnp.einsum("erf,edf->erd", hidden, down_piece, preferred_element_type=jnp.float32)
    expert_rows = expert_sum.astype(jnp.bfloat16)
    returned = exchange_in_pieces(expert_rows, "ep", 2, 1, 0)
    returned_rows = returned.reshape(EXPERTS * CAP, returned.shape[2])
    combined = jnp.zeros((normed.shape[0], normed.shape[1]), jnp.float32)
    for route_index in range(TOP):
        picking = (slots[:, route_index][:, None] == slot_index[None, :]).astype(jnp.bfloat16)
        chosen_rows = jnp.dot(picking, returned_rows, preferred_element_type=jnp.float32)
        combined = combined + route_weight[:, route_index : route_index + 1] * chosen_rows
    moe_out = combined.astype(jnp.bfloat16)
    return (mixed_sum, moe_out)


def solution(mesh):
    return jax.shard_map(
        body,
        mesh=mesh,
        in_specs=(
            P("ep", "tp"),
            P("tp"),
            P("tp", None),
            P(("ep", "tp"), None),
            P(),
            P(("ep", "tp"), None),
            P(("ep", "tp"), None),
            P("ep", None, "tp"),
            P("ep", None, "tp"),
            P("ep", None, "tp"),
        ),
        out_specs=(P(("ep", "tp"), None), P(("ep", "tp"), None)),
        check_vma=False,
    )
```

profile of v0, /device:TPU:24, one launch (start us, length us, event | category | flops | bytes accessed | tf_op | source)
XLA Modules:
  0.0 169.4 jit_solution(2128738845076339087)
XLA Ops:
  7.2 0.0 copy-start
  7.2 0.0 all-gather.2.cloned.1.call-start
  7.2 2.1 %pad_maximum_fusion.1 = bf16[64,6144]{1,0:T(8,128)(2,1)} fusion(bf16[64,2048]{1,0:T(8,128)(2,1)} %bitcast.76, bf16[64,2048]{1,0:T(8,128)(2,1)} %bitcast.77, bf16[64,2048]{1,0:T(8,128)(2,1)} %bitcast.78), kind=kLoop, calls=%fused_computation.22 | loop fusion | flops 2359296 | bytes 1572864 | tf_op jit(solution)/shard_map/concatenate | solution.py:21
  9.3 0.0 all-gather.2.cloned.1.call-update
  9.3 0.0 copy-start.4
  9.3 0.0 reduce-scatter.2.cloned.1.call-start
  9.4 0.8 slice.66
  10.2 3.4 %collective-permute-start = (bf16[15,64]{0,1:T(8,128)(2,1)S(1)}, bf16[15,64]{0,1:T(8,128)(2,1)S(1)}, u32[]{:S(2)}, u32[]{:S(2)}) collective-permute-start(bf16[15,64]{0,1:T(8,128)(2,1)S(1)} %slice.66), channel_id=1, source_target_pairs={{0,16},{16,32},{32,48},{48,64},{64,80},{80,96},{96,112},{112,128},... | collective-permute-start | bytes 5768 | tf_op jit(solution)/shard_map/ppermute | solution.py:16
  13.7 4.3 %collective-permute-done = bf16[15,64]{0,1:T(8,128)(2,1)S(1)} collective-permute-done((bf16[15,64]{0,1:T(8,128)(2,1)S(1)}, bf16[15,64]{0,1:T(8,128)(2,1)S(1)}, u32[]{:S(2)}, u32[]{:S(2)}) %collective-permute-start) | collective-permute-done | bytes 1952 | tf_op jit(solution)/shard_map/ppermute | solution.py:16
  17.9 1.1 maximum_convert_fusion
  19.0 0.2 slice_add_fusion.2
  19.2 0.2 slice_add_fusion.1
  19.5 0.2 slice_add_fusion
  19.7 0.0 copy-done
  19.7 0.0 copy-done.4
  19.7 6.5 %convolution_convert_fusion = bf16[2048,2048]{1,0:T(8,128)(2,1)} fusion(bf16[64,2048]{1,0:T(8,128)(2,1)S(1)} %copy-done, f32[2063,64]{0,1:T(8,128)S(1)} %maximum_convert_fusion, f32[2062,64]{0,1:T(8,128)S(1)} %slice_add_fusion.2, f32[2060,64]{0,1:T(8,128)S(1)} %slice_add_fusion.1, f32[2056,64]{0,1:T(8,128)S(1)} %slice_add_fusion, f32[64]{0:T(128)S(1)} %copy-done.4, ...), kind=kOutput, calls=%fused_computation | convolution fusion | flops 542507008 | bytes 11283456 | tf_op jit(solution)/shard_map/dot_general | solution.py:108
  26.2 0.0 copy-start.3
  26.2 0.0 copy-start.1
  26.2 0.0 copy-start.2
  26.2 0.0 reduce-scatter.2.cloned.1.call-update
  26.2 0.7 copy-done.3
  26.9 0.1 copy.29
  27.0 0.1 eq.138
  27.1 0.1 eq.134
  27.3 1.2 reduce-window.6
  28.5 0.2 slice_reduce_fusion
  28.7 0.1 fusion.35
  28.8 0.1 reduce_sum.21
  29.0 0.1 copy.32
  29.0 0.0 copy-done.1
  29.0 0.3 fusion.6
  29.4 0.0 copy-done.2
  29.4 1.1 convolution_convert_fusion.1
  30.5 41.2 %all_to_all.19 = bf16[16,48,2048]{2,1,0:T(8,128)(2,1)S(1)} all-to-all(bf16[16,48,2048]{2,1,0:T(8,128)(2,1)S(1)} %bitcast.72), channel_id=1, replica_groups=mesh['ep'=16,'tp'=16] {'ep'}, dimensions={0} | all-to-all | bytes 6291456 | tf_op jit(solution)/shard_map/all_to_all | solution.py:123
  71.7 17.0 %all-gather.2.cloned.1.call-done = bf16[1024,6144]{1,0:T(8,128)(2,1)} async-done(((bf16[64,6144]{1,0:T(8,128)(2,1)}), bf16[1024,6144]{1,0:T(8,128)(2,1)}) %all-gather.2.cloned.1.call-update) | async-done | bytes 12582928 | tf_op jit(solution)/shard_map/all_gather | solution.py:22
  88.7 5.4 %fusion.1 = f32[768,1024]{1,0:T(8,128)S(1)} fusion(bf16[768,2048]{1,0:T(8,128)(2,1)S(1)} %bitcast.73, bf16[1024,6144]{1,0:T(8,128)(2,1)} %all-gather.2.cloned.1.call-done), kind=kOutput, calls=%fused_computation.4 | convolution fusion | flops 3221225472 | bytes 10485760 | tf_op jit(solution)/shard_map/erd,edf->erf/dot_general | solution.py:128
  94.1 0.4 copy-done.6
  94.6 3.9 %multiply_convert_fusion = bf16[768,1024]{1,0:T(8,128)(2,1)S(1)} fusion(f32[768,1024]{1,0:T(8,128)S(1)} %fusion.1, bf16[768,2048]{1,0:T(8,128)(2,1)S(1)} %bitcast.74, bf16[1024,6144]{1,0:T(8,128)(2,1)S(1)} %copy-done.6), kind=kOutput, calls=%fused_computation.10 | convolution fusion | flops 3225944064 | bytes 12058624 | tf_op jit(solution)/shard_map/erd,edf->erf/dot_general | solution.py:127
  98.4 3.6 %fusion.3 = bf16[768,2048]{1,0:T(8,128)(2,1)S(1)} fusion(bf16[768,1024]{1,0:T(8,128)(2,1)S(1)} %multiply_convert_fusion, bf16[1024,6144]{1,0:T(8,128)(2,1)S(1)} %copy-done.6), kind=kOutput, calls=%fused_computation.7 | convolution fusion | flops 3222798336 | bytes 8912896 | tf_op jit(solution)/shard_map/erf,edf->erd/dot_general | solution.py:130
  102.1 1.4 fusion.38
  103.5 28.0 %all_to_all.20 = bf16[16,1,24,2048]{3,2,1,0:T(8,128)(2,1)S(1)} all-to-all(bf16[16,1,24,2048]{3,2,1,0:T(8,128)(2,1)S(1)} %get-tuple-element.2), channel_id=1, replica_groups=mesh['ep'=16,'tp'=16] {'ep'}, dimensions={0} | all-to-all | bytes 3145728 | tf_op jit(solution)/shard_map/all_to_all | solution.py:52
  131.5 6.0 %all-to-all-start.2 = ((bf16[16,1,24,2048]{3,2,1,0:T(8,128)(2,1)}), bf16[16,1,24,2048]{3,2,1,0:T(8,128)(2,1)S(1)}, u32[]{:S(2)}, u32[]{:S(2)}) async-start(bf16[16,1,24,2048]{3,2,1,0:T(8,128)(2,1)} %get-tuple-element.3), calls=%async_computation.3 | async-start | bytes 3145728 | tf_op jit(solution)/shard_map/all_to_all | solution.py:52
  137.4 0.0 copy-done.5
  137.5 21.1 %all-to-all-done.2 = bf16[16,1,24,2048]{3,2,1,0:T(8,128)(2,1)S(1)} async-done(((bf16[16,1,24,2048]{3,2,1,0:T(8,128)(2,1)}), bf16[16,1,24,2048]{3,2,1,0:T(8,128)(2,1)S(1)}, u32[]{:S(2)}, u32[]{:S(2)}) %all-to-all-start.2) | async-done | bytes 1572896 | tf_op jit(solution)/shard_map/all_to_all | solution.py:52
  158.5 0.4 pad_maximum_fusion
  158.9 1.1 convolution_multiply_fusion.1
  160.0 2.1 %fusion.5 = bf16[256,2048]{1,0:T(8,128)(2,1)} fusion(f32[256,2048]{1,0:T(8,128)S(1)} %convolution_multiply_fusion.1, bf16[768,2048]{1,0:T(8,128)(2,1)S(1)} %bitcast.71, f32[256]{0:T(256)S(1)} %bitcast.81, s32[256]{0:T(256)S(1)} %bitcast.80), kind=kOutput, calls=%fused_computation.16 | convolution fusion | flops 807075840 | bytes 6293504 | tf_op jit(solution)/shard_map/dot_general | solution.py:137
  162.1 0.4 reduce-scatter.2.cloned.1.call-done
  (13 shorter events, 0.1 us)
Async XLA Ops:
  7.2 12.5 %copy-start = (bf16[64,2048]{1,0:T(8,128)(2,1)S(1)}, bf16[64,2048]{1,0:T(8,128)(2,1)}, u32[]{:S(2)}) copy-start(bf16[64,2048]{1,0:T(8,128)(2,1)} %param.12) | copy-start | bytes 786436
  7.2 81.5 %all-gather.2.cloned.1.call-start = ((), (), s32[]{:S(2)}) async-start(), calls=%async_computation.5 | async-start | bytes 13369344 | tf_op jit(solution)/shard_map/all_gather | solution.py:22
  9.3 10.4 %copy-start.4 = (f32[64]{0:T(128)S(1)}, f32[64]{0:T(128)}, u32[]{:S(2)}) copy-start(f32[64]{0:T(128)} %param.11) | copy-start | bytes 772
  9.3 153.2 %reduce-scatter.2.cloned.1.call-start = ((), (), s32[]{:S(2)}) async-start(), calls=%async_computation.4 | async-start | bytes 8912896 | tf_op jit(solution)/shard_map/reduce_scatter | solution.py:107
  10.2 7.7 %collective-permute-start = (bf16[15,64]{0,1:T(8,128)(2,1)S(1)}, bf16[15,64]{0,1:T(8,128)(2,1)S(1)}, u32[]{:S(2)}, u32[]{:S(2)}) collective-permute-start(bf16[15,64]{0,1:T(8,128)(2,1)S(1)} %slice.66), channel_id=1, source_target_pairs={{0,16},{16,32},{32,48},{48,64},{64,80},{80,96},{96,112},{112,128},... | collective-permute-start | bytes 5768 | tf_op jit(solution)/shard_map/ppermute | solution.py:16
  26.2 0.7 copy-start.3
  26.2 2.9 %copy-start.1 = (bf16[256,2048]{1,0:T(8,128)(2,1)S(1)}, bf16[256,2048]{1,0:T(8,128)(2,1)}, u32[]{:S(2)}) copy-start(bf16[256,2048]{1,0:T(8,128)(2,1)} %param.13) | copy-start | bytes 3145732
  26.2 3.2 %copy-start.2 = (f32[2048]{0:T(1024)S(1)}, f32[2048]{0:T(1024)}, u32[]{:S(2)}) copy-start(f32[2048]{0:T(1024)} %param.14) | copy-start | bytes 24580
  88.7 5.8 %copy-start.6 = (bf16[1024,6144]{1,0:T(8,128)(2,1)S(1)}, bf16[1024,6144]{1,0:T(8,128)(2,1)}, u32[]{:S(2)}) copy-start(bf16[1024,6144]{1,0:T(8,128)(2,1)} %all-gather.2.cloned.1.call-done) | copy-start | bytes 37748740
  103.5 34.0 %copy-start.5 = (f32[256,2]{0,1:T(2,128)S(1)}, f32[256,2]{0,1:T(2,128)}, u32[]{:S(2)}) copy-start(f32[256,2]{0,1:T(2,128)} %param.16) | copy-start | bytes 6148
  131.5 27.0 %all-to-all-start.2 = ((bf16[16,1,24,2048]{3,2,1,0:T(8,128)(2,1)}), bf16[16,1,24,2048]{3,2,1,0:T(8,128)(2,1)S(1)}, u32[]{:S(2)}, u32[]{:S(2)}) async-start(bf16[16,1,24,2048]{3,2,1,0:T(8,128)(2,1)} %get-tuple-element.3), calls=%async_computation.3 | async-start | bytes 3145728 | tf_op jit(solution)/shard_map/all_to_all | solution.py:52
Sparse Core Ops, SparseCore 0:
  10.4 78.2 all-gather.1
  91.8 70.6 reduce-scatter.1
where the time goes:
time: 170 us; the launch traced here: 169 us
  blocking collectives  69.2 us (41%)
  waiting for transfers between devices  42.8 us (25%)
  matrix products  23.8 us (14%)
  between operations  14.3 us (8%)
  starting transfers between devices  9.42 us (6%)
  other arithmetic  5.79 us (3%)
  local copies, waits for them, and re-layouts  4.17 us (2%)
    all_to_all x1, blocking collectives, body(): lax.all_to_all(outgoing, 'ep', split_axis=0, concat_axis=1, tiled=True)  41.2 us
    all_to_all x1, blocking collectives, exchange_in_pieces(): lax.all_to_all(section, axis, split_axis=0, concat_axis=0, tiled=True)  28 us
    all_to_all x1, waiting for transfers between devices, exchange_in_pieces(): lax.all_to_all(section, axis, split_axis=0, concat_axis=0, tiled=True)  21.1 us
    all_gather x1, waiting for transfers between devices, gather_turned(): lax.all_gather(both, axis, axis=0, tiled=True)  17 us
    dot_general x1, matrix products, body(): jnp.dot(pooled, mix_weight, preferred_element_type=jnp.float32)  6.48 us
    all_to_all x1, starting transfers between devices, exchange_in_pieces(): lax.all_to_all(section, axis, split_axis=0, concat_axis=0, tiled=True)  5.95 us
    dot_general x1, matrix products, body(): jnp.einsum('erd,edf->erf', arrived, up_piece, preferred_element_type=jnp....  5.42 us
    ppermute x1, waiting for transfers between devices, from_behind(): return lax.ppermute(shard, axis, pairs)  4.26 us
  transfers between devices with their start and end apart: 4, of which 4 were waited for; matrix products, arithmetic and copies ran while one was open for 18% of the time, Pallas kernels for 0%

commit v1 on v0

--- a/solution.py
+++ b/solution.py
@@ -120,7 +120,10 @@
     ).astype(jnp.bfloat16)
     outgoing = jnp.dot(placing, normed, preferred_element_type=jnp.float32).astype(jnp.bfloat16)
     outgoing = outgoing.reshape(EXPERTS, CAP, normed.shape[1])
-    arrived = lax.all_to_all(outgoing, "ep", split_axis=0, concat_axis=1, tiled=True)
+    arrived = jnp.concatenate(
+        lax.all_to_all(jnp.stack(jnp.split(outgoing, lax.axis_size("ep"), axis=0)), "ep", 0, 0),
+        axis=1,
+    )
     gate_piece, up_piece, down_piece = gather_turned(
         (gate_weight, up_weight, down_weight), "tp", (2, 2, 2)
     )

time: 170 us -> 170 us (level)
  waiting for transfers between devices: 42.8 us -> 28.5 us
  local copies, waits for them, and re-layouts: 4.17 us -> 15.4 us
  blocking collectives: 69.2 us -> 72 us
    unnamed x15 -> x32, local copies, waits for them, and re-layouts: 1.23 us -> 11.7 us
    all_gather x1, waiting for transfers between devices: 17 us -> 6.94 us  [gather_turned(): lax.all_gather(both, axis, axis=0, tiled=True)]
    ppermute x1, waiting for transfers between devices: 4.26 us -> 0.01 us  [from_behind(): return lax.ppermute(shard, axis, pairs)]
    all_to_all x1, blocking collectives: 41.2 us -> 44 us  [body(): lax.all_to_all(jnp.stack(jnp.split(outgoing, lax.axis_size('ep'), axis=0)...]
  transfers between devices with their start and end apart: 4 -> 4, of which waited for: 4 -> 3; matrix products, arithmetic and copies ran while one was open for 18% -> 25% of each run, Pallas kernels for 0% -> 0%
where the time goes in v1:
time: 170 us; the launch traced here: 169 us
  blocking collectives  72 us (42%)
  waiting for transfers between devices  28.5 us (17%)
  matrix products  24.8 us (15%)
  local copies, waits for them, and re-layouts  15.4 us (9%)
  between operations  14.3 us (8%)
  starting transfers between devices  9.42 us (6%)
  other arithmetic  4.91 us (3%)
    all_to_all x1, blocking collectives, body(): lax.all_to_all(jnp.stack(jnp.split(outgoing, lax.axis_size('ep'), axis=0)...  44 us
    all_to_all x1, blocking collectives, exchange_in_pieces(): lax.all_to_all(section, axis, split_axis=0, concat_axis=0, tiled=True)  28 us
    all_to_all x1, waiting for transfers between devices, exchange_in_pieces(): lax.all_to_all(section, axis, split_axis=0, concat_axis=0, tiled=True)  21.1 us
    unnamed x32, local copies, waits for them, and re-layouts  11.7 us
    all_gather x1, waiting for transfers between devices, gather_turned(): lax.all_gather(both, axis, axis=0, tiled=True)  6.94 us
    dot_general x1, matrix products, body(): jnp.dot(pooled, mix_weight, preferred_element_type=jnp.float32)  6.38 us
    all_to_all x1, starting transfers between devices, exchange_in_pieces(): lax.all_to_all(section, axis, split_axis=0, concat_axis=0, tiled=True)  5.95 us
    dot_general x1, matrix products, body(): jnp.einsum('erd,edf->erf', arrived, up_piece, preferred_element_type=jnp....  5.42 us
  transfers between devices with their start and end apart: 4, of which 3 were waited for; matrix products, arithmetic and copies ran while one was open for 25% of the time, Pallas kernels for 0%

profile of v1, /device:TPU:24, one launch (start us, length us, event | category | flops | bytes accessed | tf_op | source)
XLA Modules:
  0.0 169.4 jit_solution(15237307475381436052)
XLA Ops:
  7.3 2.1 %pad_maximum_fusion.1 = bf16[64,6144]{1,0:T(8,128)(2,1)} fusion(bf16[64,2048]{1,0:T(8,128)(2,1)} %bitcast.138, bf16[64,2048]{1,0:T(8,128)(2,1)} %bitcast.139, bf16[64,2048]{1,0:T(8,128)(2,1)} %bitcast.140), kind=kLoop, calls=%fused_computation.22 | loop fusion | flops 2359296 | bytes 1572864 | tf_op jit(solution)/shard_map/concatenate | solution.py:21
  9.5 0.8 slice.82
  10.3 3.4 %collective-permute-start = (bf16[15,64]{0,1:T(8,128)(2,1)S(1)}, bf16[15,64]{0,1:T(8,128)(2,1)S(1)}, u32[]{:S(2)}, u32[]{:S(2)}) collective-permute-start(bf16[15,64]{0,1:T(8,128)(2,1)S(1)} %slice.82), channel_id=1, source_target_pairs={{0,16},{16,32},{32,48},{48,64},{64,80},{80,96},{96,112},{112,128},... | collective-permute-start | bytes 5768 | tf_op jit(solution)/shard_map/ppermute | solution.py:16
  13.7 0.8 copy.29
  14.5 0.1 eq.138
  14.6 0.1 eq.134
  14.8 1.2 reduce-window.6
  15.9 0.2 slice_reduce_fusion
  16.2 0.1 fusion.51
  16.3 0.1 reduce_sum.21
  16.4 0.1 copy.32
  16.6 0.3 fusion.6
  16.9 2.4 %convolution_convert_fusion.1 = bf16[768,2048]{1,0:T(8,128)(2,1)S(1)} fusion(bf16[256,2048]{1,0:T(8,128)(2,1)} %param.13, f32[2048]{0:T(1024)S(1)} %copy-done.3, f32[256]{0:T(256)S(1)} %add_rsqrt_fusion, s32[256]{0:T(256)S(1)} %bitcast.141, s32[256]{0:T(256)S(1)} %bitcast.144), kind=kOutput, calls=%fused_computation.8 | convolution fusion | flops 809566208 | bytes 4205568 | tf_op jit(solution)/shard_map/dot_general | solution.py:121
  19.4 0.7 fusion.48
  20.1 0.1 maximum_convert_fusion
  20.2 0.2 slice_add_fusion.2
  20.4 0.2 slice_add_fusion.1
  20.7 0.2 slice_add_fusion
  20.9 6.4 %convolution_convert_fusion = bf16[2048,2048]{1,0:T(8,128)(2,1)} fusion(bf16[64,2048]{1,0:T(8,128)(2,1)S(1)} %copy-done, f32[2063,64]{0,1:T(8,128)S(1)} %maximum_convert_fusion, f32[2062,64]{0,1:T(8,128)S(1)} %slice_add_fusion.2, f32[2060,64]{0,1:T(8,128)S(1)} %slice_add_fusion.1, f32[2056,64]{0,1:T(8,128)S(1)} %slice_add_fusion, f32[64]{0:T(128)S(1)} %copy-done.5, ...), kind=kOutput, calls=%fused_computation | convolution fusion | flops 542507008 | bytes 11283456 | tf_op jit(solution)/shard_map/dot_general | solution.py:108
  27.3 0.7 fusion.47
  28.0 0.7 fusion.46
  28.7 0.7 fusion.45
  29.4 0.7 fusion.44
  30.1 0.7 fusion.43
  30.8 0.7 fusion.42
  31.5 0.7 fusion.41
  32.2 0.7 fusion.40
  32.9 0.7 fusion.39
  33.6 0.7 fusion.38
  34.3 0.7 fusion.37
  35.0 0.7 fusion.36
  35.7 0.7 fusion.35
  36.4 0.7 fusion.34
  37.1 0.7 fusion.33
  37.8 44.0 %all_to_all.15 = bf16[16,1,48,2048]{3,2,1,0:T(8,128)(2,1)S(1)} all-to-all(bf16[16,1,48,2048]{3,2,1,0:T(8,128)(2,1)} %fusion.33), channel_id=1, replica_groups=mesh['ep'=16,'tp'=16] {'ep'}, dimensions={0} | all-to-all | bytes 6291456 | tf_op jit(solution)/shard_map/all_to_all | solution.py:124
  81.8 6.9 %all-gather.2.cloned.1.call-done = bf16[1024,6144]{1,0:T(8,128)(2,1)} async-done(((bf16[64,6144]{1,0:T(8,128)(2,1)}), bf16[1024,6144]{1,0:T(8,128)(2,1)}) %all-gather.2.cloned.1.call-update) | async-done | bytes 12582928 | tf_op jit(solution)/shard_map/all_gather | solution.py:22
  88.8 5.4 %fusion.1 = f32[768,1024]{1,0:T(8,128)S(1)} fusion(bf16[768,2048]{1,0:T(8,128)(2,1)S(1)} %bitcast.135, bf16[1024,6144]{1,0:T(8,128)(2,1)} %all-gather.2.cloned.1.call-done), kind=kOutput, calls=%fused_computation.4 | convolution fusion | flops 3221225472 | bytes 10485760 | tf_op jit(solution)/shard_map/erd,edf->erf/dot_general | solution.py:131
  94.2 0.4 copy-done.7
  94.6 3.8 %multiply_convert_fusion = bf16[768,1024]{1,0:T(8,128)(2,1)S(1)} fusion(f32[768,1024]{1,0:T(8,128)S(1)} %fusion.1, bf16[768,2048]{1,0:T(8,128)(2,1)S(1)} %bitcast.136, bf16[1024,6144]{1,0:T(8,128)(2,1)S(1)} %copy-done.7), kind=kOutput, calls=%fused_computation.10 | convolution fusion | flops 3225944064 | bytes 12058624 | tf_op jit(solution)/shard_map/erd,edf->erf/dot_general | solution.py:130
  98.4 3.6 %fusion.3 = bf16[768,2048]{1,0:T(8,128)(2,1)S(1)} fusion(bf16[768,1024]{1,0:T(8,128)(2,1)S(1)} %multiply_convert_fusion, bf16[1024,6144]{1,0:T(8,128)(2,1)S(1)} %copy-done.7), kind=kOutput, calls=%fused_computation.7 | convolution fusion | flops 3222798336 | bytes 8912896 | tf_op jit(solution)/shard_map/erf,edf->erd/dot_general | solution.py:133
  102.1 1.4 fusion.54
  103.5 28.0 %all_to_all.16 = bf16[16,1,24,2048]{3,2,1,0:T(8,128)(2,1)S(1)} all-to-all(bf16[16,1,24,2048]{3,2,1,0:T(8,128)(2,1)S(1)} %get-tuple-element.2), channel_id=1, replica_groups=mesh['ep'=16,'tp'=16] {'ep'}, dimensions={0} | all-to-all | bytes 3145728 | tf_op jit(solution)/shard_map/all_to_all | solution.py:52
  131.5 6.0 %all-to-all-start.2 = ((bf16[16,1,24,2048]{3,2,1,0:T(8,128)(2,1)}), bf16[16,1,24,2048]{3,2,1,0:T(8,128)(2,1)S(1)}, u32[]{:S(2)}, u32[]{:S(2)}) async-start(bf16[16,1,24,2048]{3,2,1,0:T(8,128)(2,1)} %get-tuple-element.3), calls=%async_computation.3 | async-start | bytes 3145728 | tf_op jit(solution)/shard_map/all_to_all | solution.py:52
  137.4 21.1 %all-to-all-done.2 = bf16[16,1,24,2048]{3,2,1,0:T(8,128)(2,1)S(1)} async-done(((bf16[16,1,24,2048]{3,2,1,0:T(8,128)(2,1)}), bf16[16,1,24,2048]{3,2,1,0:T(8,128)(2,1)S(1)}, u32[]{:S(2)}, u32[]{:S(2)}) %all-to-all-start.2) | async-done | bytes 1572896 | tf_op jit(solution)/shard_map/all_to_all | solution.py:52
  158.5 0.4 pad_maximum_fusion
  158.9 1.1 convolution_multiply_fusion.1
  160.0 2.1 %fusion.5 = bf16[256,2048]{1,0:T(8,128)(2,1)} fusion(f32[256,2048]{1,0:T(8,128)S(1)} %convolution_multiply_fusion.1, bf16[768,2048]{1,0:T(8,128)(2,1)S(1)} %bitcast.134, f32[256]{0:T(256)S(1)} %bitcast.143, s32[256]{0:T(256)S(1)} %bitcast.142), kind=kOutput, calls=%fused_computation.16 | convolution fusion | flops 807075840 | bytes 6293504 | tf_op jit(solution)/shard_map/dot_general | solution.py:140
  162.1 0.5 reduce-scatter.2.cloned.1.call-done
  (31 shorter events, 0.3 us)
Async XLA Ops:
  7.2 13.7 %copy-start = (bf16[64,2048]{1,0:T(8,128)(2,1)S(1)}, bf16[64,2048]{1,0:T(8,128)(2,1)}, u32[]{:S(2)}) copy-start(bf16[64,2048]{1,0:T(8,128)(2,1)} %param.12) | copy-start | bytes 786436
  7.2 9.7 %copy-start.4 = (s32[256,2]{0,1:T(2,128)S(1)}, s32[256,2]{0,1:T(2,128)}, u32[]{:S(2)}) copy-start(s32[256,2]{0,1:T(2,128)} %param.15) | copy-start | bytes 6148
  7.2 9.4 %copy-start.1 = (bf16[256,2048]{1,0:T(8,128)(2,1)S(1)}, bf16[256,2048]{1,0:T(8,128)(2,1)}, u32[]{:S(2)}) copy-start(bf16[256,2048]{1,0:T(8,128)(2,1)} %param.13) | copy-start | bytes 3145732
  7.2 9.7 %copy-start.3 = (f32[2048]{0:T(1024)S(1)}, f32[2048]{0:T(1024)}, u32[]{:S(2)}) copy-start(f32[2048]{0:T(1024)} %param.14) | copy-start | bytes 24580
  7.2 81.5 %all-gather.2.cloned.1.call-start = ((), (), s32[]{:S(2)}) async-start(), calls=%async_computation.5 | async-start | bytes 13369344 | tf_op jit(solution)/shard_map/all_gather | solution.py:22
  9.4 153.2 %reduce-scatter.2.cloned.1.call-start = ((), (), s32[]{:S(2)}) async-start(), calls=%async_computation.4 | async-start | bytes 8912896 | tf_op jit(solution)/shard_map/reduce_scatter | solution.py:107
  10.3 9.8 %collective-permute-start = (bf16[15,64]{0,1:T(8,128)(2,1)S(1)}, bf16[15,64]{0,1:T(8,128)(2,1)S(1)}, u32[]{:S(2)}, u32[]{:S(2)}) collective-permute-start(bf16[15,64]{0,1:T(8,128)(2,1)S(1)} %slice.82), channel_id=1, source_target_pairs={{0,16},{16,32},{32,48},{48,64},{64,80},{80,96},{96,112},{112,128},... | collective-permute-start | bytes 5768 | tf_op jit(solution)/shard_map/ppermute | solution.py:16
  16.9 3.1 %copy-start.2 = (bf16[2048,64]{0,1:T(8,128)(2,1)S(1)}, bf16[2048,64]{0,1:T(8,128)(2,1)}, u32[]{:S(2)}) copy-start(bf16[2048,64]{0,1:T(8,128)(2,1)} %param.10) | copy-start | bytes 786436
  19.3 1.5 copy-start.5
  88.7 5.8 %copy-start.7 = (bf16[1024,6144]{1,0:T(8,128)(2,1)S(1)}, bf16[1024,6144]{1,0:T(8,128)(2,1)}, u32[]{:S(2)}) copy-start(bf16[1024,6144]{1,0:T(8,128)(2,1)} %all-gather.2.cloned.1.call-done) | copy-start | bytes 37748740
  103.5 34.0 %copy-start.6 = (f32[256,2]{0,1:T(2,128)S(1)}, f32[256,2]{0,1:T(2,128)}, u32[]{:S(2)}) copy-start(f32[256,2]{0,1:T(2,128)} %param.16) | copy-start | bytes 6148
  131.5 27.0 %all-to-all-start.2 = ((bf16[16,1,24,2048]{3,2,1,0:T(8,128)(2,1)}), bf16[16,1,24,2048]{3,2,1,0:T(8,128)(2,1)S(1)}, u32[]{:S(2)}, u32[]{:S(2)}) async-start(bf16[16,1,24,2048]{3,2,1,0:T(8,128)(2,1)} %get-tuple-element.3), calls=%async_computation.3 | async-start | bytes 3145728 | tf_op jit(solution)/shard_map/all_to_all | solution.py:52
Sparse Core Ops, SparseCore 0:
  10.4 78.2 all-gather.1
  91.9 70.6 reduce-scatter.1
